TPU v7x, 256 devices: a 4x2x16 block of a 4x16x16 slice. The times are simulated.
256 devices in a mesh: grp: 2 (over y), kv: 16 (over z), tp: 8 (over x, core).
Axes of the slice: x: 4, y: 2, z: 16, core: 2. Of those that a mesh axis runs over, the one named last changes fastest.
The devices are a block of a 4x16x16 slice.
Arguments:
- piece_tokens: bfloat16 [8192, 2048], P(('grp', 'kv')), parts along dimension 0, may hold values from -6 to 6
- dec_tokens: bfloat16 [128, 2048], P(('grp', 'kv')), parts along dimension 0, may hold values from -6 to 6
- norm_gain: float32 [2048], replicated, may hold values from 0.1 to 1.9
- query_weight: bfloat16 [2048, 1024], P(None, 'tp'), may hold values from -0.125 to 0.125
- key_weight: bfloat16 [2048, 1024], P(None, 'tp'), may hold values from -0.125 to 0.125
- value_weight: bfloat16 [2048, 1024], P(None, 'tp'), may hold values from -0.125 to 0.125
- forget_weight: bfloat16 [2048, 8], P(None, 'tp'), may hold values from -0.125 to 0.125
- forget_bias: float32 [8], P('tp'), may hold values from 3 to 13
- out_weight: bfloat16 [1024, 2048], P(None, 'tp'), may hold values from -0.1875 to 0.1875
- cache_keys: bfloat16 [131072, 1024], P(('grp', 'kv'), 'tp'), parts along dimension 0, may hold values from -480 to 480
- cache_values: bfloat16 [131072, 1024], P(('grp', 'kv'), 'tp'), parts along dimension 0, may hold values from -6 to 6
- cache_gates: float32 [8, 131072], P('tp', ('grp', 'kv')), parts along dimension 1, as said below
- dec_keys: bfloat16 [128, 2048, 1024], P(('grp', 'kv'), None, 'tp'), parts along dimension 0, may hold values from -480 to 480
- dec_values: bfloat16 [128, 2048, 1024], P(('grp', 'kv'), None, 'tp'), parts along dimension 0, may hold values from -6 to 6
- dec_gates: float32 [128, 8, 2048], P(('grp', 'kv'), 'tp'), parts along dimension 0, as said below
- dec_lengths: int32 [128], P(('grp', 'kv')), parts along dimension 0, may hold values from 1 to 2048, as said below
Outputs:
- piece_out: bfloat16 [8192, 2048], P(('grp', 'kv'), 'tp'), parts along dimension 0
- dec_out: bfloat16 [128, 2048], P(('grp', 'kv'), 'tp'), parts along dimension 0
- piece_keys: bfloat16 [8192, 1024], P(('grp', 'kv'), 'tp'), parts along dimension 0
- piece_values: bfloat16 [8192, 1024], P(('grp', 'kv'), 'tp'), parts along dimension 0
There are 2 independent parts, one for each index of `grp`. A program takes and returns all parts, laid end to end along the dimension named above; an argument that names none is the same for every part. Nothing has to cross between parts.
Inputs may be any that keep to these rules, and one draw needn't show every extreme that they name: cache_gates never falls along positions and is 0 at the last cached position. dec_gates never falls along a sequence's live slots and is 0 at its last live slot and beyond. Slots 0 to dec_lengths[b] - 1 of sequence b are live; some sequence has exactly 2048.
All inputs are finite; a program needn't handle non-finite values.
Results may differ from a plain program's by a relative error of at most 0.015.
Values may be sent and summed in bfloat16 or wider, within the bound.
A program may use at most 64 MiB of HBM per device.

v0:
```python
import math
import jax
import jax.numpy as jnp
from jax import lax
from jax.sharding import PartitionSpec as P

norm_eps = 1e-05


def from_everyone(shard, axis):
    devices = lax.axis_size(axis)
    return lax.all_to_all(
        jnp.broadcast_to(shard[None], (devices, *shard.shape)), axis, 0, 0, tiled=True
    )


def folded_in_pairs(pieces, combine):
    while len(jax.tree.leaves(pieces)[0]) > 1:
        pieces = jax.vmap(combine)(*(pieces[side::2] for side in (0, 1)))
    return pieces[0]


def prefix(shard, axis, combine, identity):
    devices, mine = (lax.axis_size(axis), lax.axis_index(axis))
    passed = jnp.arange(devices) < mine

    def kept(part, zero, own):
        part = jnp.where(
            passed.reshape(-1, *(1 for _ in own.shape)), part, jnp.asarray(zero, own.dtype)
        )
        return part

    pieces = from_everyone(shard, axis)
    return folded_in_pairs(kept(pieces, identity, shard), combine)


def taken_together(shard, axis):
    everything = from_everyone(shard, axis)
    return jnp.max(everything, axis=0)


def cut_along(shard, dim, devices):
    shape = shard.shape
    parts = shard.reshape(*shape[:dim], devices, shape[dim] // devices, *shape[dim + 1 :])
    return jnp.moveaxis(parts, dim, 0)


def sent_and_summed(shard, axis, dim):
    devices = lax.axis_size(axis)
    parts = lax.all_to_all(cut_along(shard, dim, devices), axis, 0, 0, tiled=True)
    return jnp.sum(parts.astype(jnp.float32), axis=0)


def sent_and_summed_2(shard, axis, dim):
    devices = lax.axis_size(axis)
    parts = lax.all_to_all(cut_along(shard, dim, devices), axis, 0, 0, tiled=True)
    return jnp.sum(parts, axis=0)


def sent_together(arrays, axis, dim, along):
    both = jnp.concatenate(arrays, axis=along)
    result, at, finished = (lax.all_gather(both, axis, axis=dim, tiled=True), 0, [])
    for a in arrays:
        finished.append(lax.slice_in_dim(result, at, at + a.shape[along], axis=along))
        at += a.shape[along]
    return tuple(finished)


def rms_norm(tokens, norm_gain):
    values = tokens.astype(jnp.float32)
    factor = lax.rsqrt(jnp.mean(values * values, axis=-1, keepdims=True) + norm_eps)
    return (values * factor * norm_gain).astype(jnp.bfloat16)


def project(tokens, norm_gain, query_weight, key_weight, value_weight, forget_weight, forget_bias):
    normed = rms_norm(tokens, norm_gain)
    queries = jnp.dot(normed, query_weight, preferred_element_type=jnp.float32).astype(jnp.bfloat16)
    key_rows = jnp.dot(normed, key_weight, preferred_element_type=jnp.float32).astype(jnp.bfloat16)
    value_rows = jnp.dot(normed, value_weight, preferred_element_type=jnp.float32).astype(
        jnp.bfloat16
    )
    log_gates = jax.nn.log_sigmoid(
        jnp.dot(normed, forget_weight, preferred_element_type=jnp.float32) + forget_bias
    )
    return (queries, key_rows, value_rows, log_gates)


def add_pair(earlier_sum, later_sum):
    return earlier_sum + later_sum


def shards(
    piece_tokens,
    dec_tokens,
    norm_gain,
    query_weight,
    key_weight,
    value_weight,
    forget_weight,
    forget_bias,
    out_weight,
    cache_keys,
    cache_values,
    cache_gates,
    dec_keys,
    dec_values,
    dec_gates,
    dec_lengths,
):
    piece_count = piece_tokens.shape[0]
    local_heads = forget_weight.shape[1]
    head_size = query_weight.shape[1] // local_heads
    score_scale = head_size ** (-0.5)
    piece_parts = project(
        piece_tokens, norm_gain, query_weight, key_weight, value_weight, forget_weight, forget_bias
    )
    dec_parts = project(
        dec_tokens, norm_gain, query_weight, key_weight, value_weight, forget_weight, forget_bias
    )
    piece_queries, piece_keys, piece_values, piece_gates = piece_parts
    dec_queries, dec_new_keys, dec_new_values, dec_gate_now = dec_parts
    running = jnp.cumsum(piece_gates, axis=0)
    offset = prefix(running[-1], "kv", add_pair, jnp.zeros_like(running[-1]))
    piece_bias = -(running + offset[None, :]).T
    all_queries = lax.all_gather(piece_queries, "kv", axis=0, tiled=True)
    shard_index = lax.axis_index("kv")
    key_order = shard_index * piece_count + jnp.arange(piece_count, dtype=jnp.int32)
    cache_rows = cache_keys.shape[0]
    cache_key_heads = cache_keys.reshape(cache_rows, local_heads, head_size)
    cache_value_heads = cache_values.reshape(cache_rows, local_heads, head_size)
    piece_key_heads = piece_keys.reshape(piece_count, local_heads, head_size)
    piece_value_heads = piece_values.reshape(piece_count, local_heads, head_size)
    total_rows = all_queries.shape[0]
    block_rows = math.gcd(total_rows, 512)
    block_count = total_rows // block_rows
    query_blocks = all_queries.reshape(block_count, block_rows, local_heads, head_size)
    block_starts = jnp.arange(block_count, dtype=jnp.int32) * block_rows

    def block_terms(inputs):
        query_block, first_row = inputs
        cache_scores = (
            jnp.einsum(
                "qhd,khd->hqk", query_block, cache_key_heads, preferred_element_type=jnp.float32
            )
            * score_scale
            + cache_gates[:, None, :]
        )
        piece_scores = (
            jnp.einsum(
                "qhd,khd->hqk", query_block, piece_key_heads, preferred_element_type=jnp.float32
            )
            * score_scale
            + piece_bias[:, None, :]
        )
        query_order = first_row + jnp.arange(block_rows, dtype=jnp.int32)
        visible = key_order[None, :] <= query_order[:, None]
        piece_scores = jnp.where(visible[None], piece_scores, -jnp.inf)
        local_max = jnp.maximum(jnp.max(cache_scores, axis=-1), jnp.max(piece_scores, axis=-1))
        cache_exp = jnp.exp(cache_scores - local_max[:, :, None])
        piece_exp = jnp.exp(piece_scores - local_max[:, :, None])
        numerator = jnp.einsum(
            "hqk,khd->qhd",
            cache_exp.astype(jnp.bfloat16),
            cache_value_heads,
            preferred_element_type=jnp.float32,
        )
        numerator = numerator + jnp.einsum(
            "hqk,khd->qhd",
            piece_exp.astype(jnp.bfloat16),
            piece_value_heads,
            preferred_element_type=jnp.float32,
        )
        denominator = jnp.sum(cache_exp, axis=-1) + jnp.sum(piece_exp, axis=-1)
        return (numerator.astype(jnp.bfloat16), denominator.T, local_max.T)

    numerators, denominators, local_maxima = lax.map(block_terms, (query_blocks, block_starts))
    numerators = numerators.reshape(total_rows, local_heads, head_size)
    denominators = denominators.reshape(total_rows, local_heads)
    local_maxima = local_maxima.reshape(total_rows, local_heads)
    maxima = taken_together(local_maxima, "kv")
    factors = jnp.exp(local_maxima - maxima)
    scaled = (numerators.astype(jnp.float32) * factors[:, :, None]).astype(jnp.bfloat16)
    rounded = (
        lax.optimization_barrier(scaled)
        .astype(jnp.float32)
        .reshape(total_rows, local_heads * head_size)
    )
    denominators = denominators * factors
    own_numer = sent_and_summed(rounded.astype(jnp.bfloat16), "kv", 0)
    own_denom = sent_and_summed_2(denominators, "kv", 0)
    piece_attention = (
        own_numer.reshape(piece_count, local_heads, head_size) / own_denom[:, :, None]
    ).astype(jnp.bfloat16)
    piece_attention = piece_attention.reshape(piece_count, local_heads * head_size)
    dec_count = dec_tokens.shape[0]
    dec_span = dec_keys.shape[1]
    dec_query_heads = dec_queries.reshape(dec_count, local_heads, head_size)
    new_key_heads = dec_new_keys.reshape(dec_count, local_heads, head_size)
    new_value_heads = dec_new_values.reshape(dec_count, local_heads, head_size)
    dec_key_heads = dec_keys.reshape(dec_count, dec_span, local_heads, head_size)
    dec_value_heads = dec_values.reshape(dec_count, dec_span, local_heads, head_size)
    cached = (
        jnp.einsum(
            "bhd,bkhd->bhk", dec_query_heads, dec_key_heads, preferred_element_type=jnp.float32
        )
        * score_scale
    )
    cached = cached + dec_gates + dec_gate_now[:, :, None]
    live_slots = jnp.arange(dec_span, dtype=jnp.int32)[None, :] < dec_lengths[:, None]
    cached = jnp.where(live_slots[:, None, :], cached, -jnp.inf)
    own_score = (
        jnp.sum(dec_query_heads.astype(jnp.float32) * new_key_heads.astype(jnp.float32), axis=-1)
        * score_scale
    )
    row_top = jnp.maximum(jnp.max(cached, axis=-1), own_score)
    cached_exp = jnp.exp(cached - row_top[:, :, None])
    own_exp = jnp.exp(own_score - row_top)
    whole_sum = jnp.sum(cached_exp, axis=-1) + own_exp
    cached_weights = (cached_exp / whole_sum[:, :, None]).astype(jnp.bfloat16)
    own_weights = (own_exp / whole_sum).astype(jnp.bfloat16)
    dec_mixed = jnp.einsum(
        "bhk,bkhd->bhd", cached_weights, dec_value_heads, preferred_element_type=jnp.float32
    )
    dec_mixed = dec_mixed + own_weights.astype(jnp.float32)[:, :, None] * new_value_heads.astype(
        jnp.float32
    )
    dec_attention = dec_mixed.astype(jnp.bfloat16).reshape(dec_count, local_heads * head_size)

    def add_columns(columns_in):
        return jnp.dot(columns_in, out_weight, preferred_element_type=jnp.float32)

    column_pair = sent_together((piece_attention, dec_attention), "tp", 1, 0)
    piece_out = add_columns(column_pair[0])
    dec_out = add_columns(column_pair[1])
    return (piece_out.astype(jnp.bfloat16), dec_out.astype(jnp.bfloat16), piece_keys, piece_values)


def solution(mesh):
    return jax.shard_map(
        shards,
        mesh=mesh,
        in_specs=(
            P(("grp", "kv"), None),
            P(("grp", "kv"), None),
            P(),
            P(None, "tp"),
            P(None, "tp"),
            P(None, "tp"),
            P(None, "tp"),
            P("tp"),
            P(None, "tp"),
            P(("grp", "kv"), "tp"),
            P(("grp", "kv"), "tp"),
            P("tp", ("grp", "kv")),
            P(("grp", "kv"), None, "tp"),
            P(("grp", "kv"), None, "tp"),
            P(("grp", "kv"), "tp", None),
            P(("grp", "kv")),
        ),
        out_specs=(
            P(("grp", "kv"), "tp"),
            P(("grp", "kv"), "tp"),
            P(("grp", "kv"), "tp"),
            P(("grp", "kv"), "tp"),
        ),
        check_vma=False,
    )
```

profile of v0, /device:TPU:161, one launch (start us, length us, event | category | flops | bytes accessed | tf_op | source)
XLA Modules:
  0.0 275.4 jit_solution(3541225993187929004)
XLA Ops:
  7.3 1.7 fusion.28
  9.0 2.5 convolution_convert_fusion.3
  16.5 22.4 %all-to-all-start = ((f32[16,1,1]{2,1,0:T(1,128)}), f32[16,1,1]{2,1,0:T(1,128)S(1)}, u32[]{:S(2)}, u32[]{:S(2)}) async-start(f32[16,1,1]{2,1,0:T(1,128)} %broadcast_in_dim.35), calls=%async_computation | async-start | bytes 16384 | tf_op jit(solution)/shard_map/all_to_all | solution.py:12
  39.0 1.9 convolution_convert_fusion.1
  40.9 1.9 convolution_convert_fusion.2
  42.8 6.4 %all-to-all-done = f32[16,1,1]{2,1,0:T(1,128)S(1)} async-done(((f32[16,1,1]{2,1,0:T(1,128)}), f32[16,1,1]{2,1,0:T(1,128)S(1)}, u32[]{:S(2)}, u32[]{:S(2)}) %all-to-all-start) | async-done | bytes 96 | tf_op jit(solution)/shard_map/all_to_all | solution.py:12
  51.8 31.0 %all-gather.2.cloned.1.call-done = bf16[4096,128]{1,0:T(8,128)(2,1)} async-done(((bf16[256,128]{1,0:T(8,128)(2,1)}), bf16[4096,128]{1,0:T(8,128)(2,1)}) %all-gather.2.cloned.1.call-update) | async-done | bytes 1048592 | tf_op jit(solution)/shard_map/all_gather | solution.py:125
  82.8 76.6 %while.15 = (s32[]{:T(128)}, bf16[8,512,1,128]{3,1,2,0:T(8,128)(2,1)}, f32[8,512,1]{1,2,0:T(1,128)S(1)}, f32[8,512,1]{1,2,0:T(1,128)S(1)}, bf16[8,512,1,128]{3,1...) while((s32[]{:T(128)}, ...), condition=%wide.region_8.9_spmd.clone, body=%wide.region_3.8_spmd.clone.sunk | while | flops 1165229824 | bytes 34173624 | solution.py:176
  84.1 1.2 fusion.97
  85.2 2.2 fusion.96
  87.5 2.1 fusion.100
  89.7 1.7 fusion.98
  93.6 1.2 fusion.97
  94.8 2.2 fusion.96
  97.1 2.1 fusion.100
  99.3 1.7 fusion.98
  103.2 1.2 fusion.97
  104.4 2.2 fusion.96
  106.7 2.1 fusion.100
  108.9 1.7 fusion.98
  112.8 1.2 fusion.97
  114.0 2.2 fusion.96
  116.2 2.1 fusion.100
  118.5 1.7 fusion.98
  122.4 1.2 fusion.97
  123.6 2.2 fusion.96
  125.8 2.1 fusion.100
  128.0 1.7 fusion.98
  132.0 1.2 fusion.97
  133.1 2.2 fusion.96
  135.4 2.1 fusion.100
  137.6 1.7 fusion.98
  141.5 1.2 fusion.97
  142.7 2.2 fusion.96
  145.0 2.1 fusion.100
  147.2 1.7 fusion.98
  152.3 2.2 fusion.96
  154.6 2.1 fusion.100
  156.8 1.7 fusion.98
  159.7 22.1 %all_to_all.24 = f32[16,4096,1]{1,2,0:T(1,128)S(1)} all-to-all(f32[16,4096,1]{1,2,0:T(1,128)S(1)} %broadcast_in_dim.37), channel_id=1, replica_groups=mesh['grp'=2,'kv'=16,'tp'=8] {'kv'}, dimensions={0} | all-to-all | bytes 524288 | tf_op jit(solution)/shard_map/all_to_all | solution.py:12
  182.6 4.2 %all-to-all-start.3 = ((f32[16,256,1]{1,2,0:T(1,128)}), f32[16,256,1]{1,2,0:T(1,128)S(1)}, u32[]{:S(2)}, u32[]{:S(2)}) async-start(f32[16,256,1]{1,2,0:T(1,128)} %bitcast.104), calls=%async_computation.3 | async-start | bytes 32768 | tf_op jit(solution)/shard_map/all_to_all | solution.py:56
  186.8 2.6 fusion.31
  189.4 7.8 %all-to-all-done.3 = f32[16,256,1]{1,2,0:T(1,128)S(1)} async-done(((f32[16,256,1]{1,2,0:T(1,128)}), f32[16,256,1]{1,2,0:T(1,128)S(1)}, u32[]{:S(2)}, u32[]{:S(2)}) %all-to-all-start.3) | async-done | bytes 16416 | tf_op jit(solution)/shard_map/all_to_all | solution.py:56
  197.2 4.5 %all-to-all-start.2 = ((bf16[16,256,128]{2,1,0:T(8,128)(2,1)}), bf16[16,256,128]{2,1,0:T(8,128)(2,1)S(1)}, u32[]{:S(2)}, u32[]{:S(2)}) async-start(bf16[16,256,128]{2,1,0:T(8,128)(2,1)} %bitcast.18), calls=%async_computation.2 | async-start | bytes 2097152 | tf_op jit(solution)/shard_map/all_to_all | solution.py:50
  202.1 1.3 convolution_convert_fusion.7
  203.4 1.3 fusion.38
  206.8 28.7 %all-to-all-done.2 = bf16[16,256,128]{2,1,0:T(8,128)(2,1)S(1)} async-done(((bf16[16,256,128]{2,1,0:T(8,128)(2,1)}), bf16[16,256,128]{2,1,0:T(8,128)(2,1)S(1)}, u32[]{:S(2)}, u32[]{:S(2)}) %all-to-all-start.2) | async-done | bytes 1048608 | tf_op jit(solution)/shard_map/all_to_all | solution.py:50
  235.7 31.1 %all_gather.7 = bf16[260,1024]{1,0:T(8,128)(2,1)S(1)} all-gather(bf16[260,128]{1,0:T(8,128)(2,1)S(1)} %pad_maximum_fusion), channel_id=1, replica_groups=mesh['grp'=2,'kv'=16,'tp'=8] {'tp'}, dimensions={1}, use_global_device_ids=true | all-gather | bytes 599040 | tf_op jit(solution)/shard_map/all_gather | solution.py:62
  (161 shorter events, 29.5 us)
Async XLA Ops:
  7.2 197.7 %copy-start = (bf16[4,2048,128]{2,1,0:T(8,128)(2,1)S(1)}, bf16[4,2048,128]{2,1,0:T(8,128)(2,1)}, u32[]{:S(2)}) copy-start(bf16[4,2048,128]{2,1,0:T(8,128)(2,1)} %param.30) | copy-start | bytes 6291460
  7.2 5.0 %copy-start.5 = (bf16[256,2048]{1,0:T(8,128)(2,1)S(1)}, bf16[256,2048]{1,0:T(8,128)(2,1)}, u32[]{:S(2)}) copy-start(bf16[256,2048]{1,0:T(8,128)(2,1)} %param.18) | copy-start | bytes 3145732
  7.2 5.0 %copy-start.9 = (f32[2048]{0:T(1024)S(1)}, f32[2048]{0:T(1024)}, u32[]{:S(2)}) copy-start(f32[2048]{0:T(1024)} %param.20) | copy-start | bytes 24580
  7.2 5.0 %copy-start.13 = (bf16[2048,1]{0,1:T(2,128)(2,1)S(1)}, bf16[2048,1]{0,1:T(2,128)(2,1)}, u32[]{:S(2)}) copy-start(bf16[2048,1]{0,1:T(2,128)(2,1)} %param.24) | copy-start | bytes 12292
  7.2 75.6 %all-gather.2.cloned.1.call-start = ((), (), s32[]{:S(2)}) async-start(), calls=%async_computation.4 | async-start | bytes 1114112 | tf_op jit(solution)/shard_map/all_gather | solution.py:125
  16.5 32.6 %all-to-all-start = ((f32[16,1,1]{2,1,0:T(1,128)}), f32[16,1,1]{2,1,0:T(1,128)S(1)}, u32[]{:S(2)}, u32[]{:S(2)}) async-start(f32[16,1,1]{2,1,0:T(1,128)} %broadcast_in_dim.35), calls=%async_computation | async-start | bytes 16384 | tf_op jit(solution)/shard_map/all_to_all | solution.py:12
  38.9 43.9 %copy-start.1 = (bf16[4096,128]{1,0:T(8,128)(2,1)S(1)}, bf16[4096,128]{1,0:T(8,128)(2,1)}, u32[]{:S(2)}) copy-start(bf16[4096,128]{1,0:T(8,128)(2,1)} %param.27) | copy-start | bytes 3145732
  39.0 43.9 %copy-start.2 = (f32[1,4096]{1,0:T(1,128)S(1)}, f32[1,4096]{1,0:T(1,128)}, u32[]{:S(2)}) copy-start(f32[1,4096]{1,0:T(1,128)} %param.29) | copy-start | bytes 49156
  87.5 2.2 copy-start.11
  97.1 2.2 copy-start.11
  106.7 2.2 copy-start.11
  116.2 2.2 copy-start.11
  125.8 2.2 copy-start.11
  135.4 2.2 copy-start.11
  145.0 2.2 copy-start.11
  154.5 2.2 copy-start.11
  159.4 37.8 %copy-start.4 = (bf16[256,1,128]{2,0,1:T(8,128)(2,1)}, bf16[256,1,128]{2,0,1:T(8,128)(2,1)S(1)}, u32[]{:S(2)}) copy-start(bf16[256,1,128]{2,0,1:T(8,128)(2,1)S(1)} %get-tuple-element.330) | copy-start | bytes 196612
  159.4 37.8 %copy-start.14 = (bf16[256,1,128]{2,0,1:T(8,128)(2,1)}, bf16[256,1,128]{2,0,1:T(8,128)(2,1)S(1)}, u32[]{:S(2)}) copy-start(bf16[256,1,128]{2,0,1:T(8,128)(2,1)S(1)} %get-tuple-element.336) | copy-start | bytes 196612
  182.6 14.7 %all-to-all-start.3 = ((f32[16,256,1]{1,2,0:T(1,128)}), f32[16,256,1]{1,2,0:T(1,128)S(1)}, u32[]{:S(2)}, u32[]{:S(2)}) async-start(f32[16,256,1]{1,2,0:T(1,128)} %bitcast.104), calls=%async_computation.3 | async-start | bytes 32768 | tf_op jit(solution)/shard_map/all_to_all | solution.py:56
  186.8 15.0 %copy-start.7 = (bf16[4,2048]{1,0:T(4,128)(2,1)S(1)}, bf16[4,2048]{1,0:T(4,128)(2,1)}, u32[]{:S(2)}) copy-start(bf16[4,2048]{1,0:T(4,128)(2,1)} %param.19) | copy-start | bytes 49156
  197.2 38.2 %all-to-all-start.2 = ((bf16[16,256,128]{2,1,0:T(8,128)(2,1)}), bf16[16,256,128]{2,1,0:T(8,128)(2,1)S(1)}, u32[]{:S(2)}, u32[]{:S(2)}) async-start(bf16[16,256,128]{2,1,0:T(8,128)(2,1)} %bitcast.18), calls=%async_computation.2 | async-start | bytes 2097152 | tf_op jit(solution)/shard_map/all_to_all | solution.py:50
  201.8 3.8 %copy-start.8 = (f32[4,1,2048]{2,1,0:T(1,128)S(1)}, f32[4,1,2048]{2,1,0:T(1,128)}, u32[]{:S(2)}) copy-start(f32[4,1,2048]{2,1,0:T(1,128)} %param.32) | copy-start | bytes 98308
  201.8 3.8 %copy-start.10 = (s32[4]{0:T(128)S(1)}, s32[4]{0:T(128)}, u32[]{:S(2)}) copy-start(s32[4]{0:T(128)} %param.33) | copy-start | bytes 52
  201.8 4.2 %copy-start.3 = (bf16[4,2048,128]{2,1,0:T(8,128)(2,1)S(1)}, bf16[4,2048,128]{2,1,0:T(8,128)(2,1)}, u32[]{:S(2)}) copy-start(bf16[4,2048,128]{2,1,0:T(8,128)(2,1)} %param.31) | copy-start | bytes 6291460
  204.9 1.6 copy-start.12
  235.5 31.3 %copy-start.6 = (bf16[1024,256]{1,0:T(8,128)(2,1)S(1)}, bf16[1024,256]{1,0:T(8,128)(2,1)}, u32[]{:S(2)}) copy-start(bf16[1024,256]{1,0:T(8,128)(2,1)} %param.26) | copy-start | bytes 1572868
Sparse Core Ops, SparseCore 0:
  11.7 71.1 all-gather.1
where the time goes:
time: 276 us; the launch traced here: 275 us
  waiting for transfers between devices  73.9 us (27%)
  matrix products  61.2 us (22%)
  blocking collectives  53.2 us (19%)
  starting transfers between devices  31.2 us (11%)
  other arithmetic  29.6 us (11%)
  between operations  17.5 us (6%)
  local copies, waits for them, and re-layouts  8.29 us (3%)
    all_gather x1, blocking collectives, sent_together(): lax.all_gather(both, axis, axis=dim, tiled=True)  31.1 us
    all_gather x1, waiting for transfers between devices, shards(): all_queries = lax.all_gather(piece_queries, 'kv', axis=0, tiled=True)  31 us
    all_to_all x1, waiting for transfers between devices, sent_and_summed(): lax.all_to_all(cut_along(shard, dim, devices), axis, 0, 0, tiled=True)  28.7 us
    all_to_all x1, starting transfers between devices, from_everyone(): lax.all_to_all(jnp.broadcast_to(shard[None], (devices, *shard.shape)), ax...  22.4 us
    all_to_all x1, blocking collectives, from_everyone(): lax.all_to_all(jnp.broadcast_to(shard[None], (devices, *shard.shape)), ax...  22.1 us
    dot_general x8, matrix products, block_terms(): jnp.einsum('qhd,khd->hqk', query_block, cache_key_heads, preferred_elemen...  18 us
    reduce_sum x16, other arithmetic, block_terms(): denominator = jnp.sum(cache_exp, axis=-1) + jnp.sum(piece_exp, axis=-1)  17.4 us
    dot_general x8, matrix products, block_terms(): jnp.einsum('hqk,khd->qhd', cache_exp.astype(jnp.bfloat16), cache_value_he...  13.8 us
  transfers between devices with their start and end apart: 4, of which 4 were waited for; matrix products, arithmetic and copies ran while one was open for 6% of the time, Pallas kernels for 0%

commit v1 on v0

--- a/solution.py
+++ b/solution.py
@@ -122,7 +122,10 @@
     running = jnp.cumsum(piece_gates, axis=0)
     offset = prefix(running[-1], "kv", add_pair, jnp.zeros_like(running[-1]))
     piece_bias = -(running + offset[None, :]).T
-    all_queries = lax.all_gather(piece_queries, "kv", axis=0, tiled=True)
+    devices_2 = lax.axis_size("kv")
+    shards_2 = jnp.stack([piece_queries for _ in range(devices_2)])
+    shards_2 = lax.all_to_all(shards_2, "kv", split_axis=0, concat_axis=0)
+    all_queries = jnp.concatenate(shards_2, axis=0)
     shard_index = lax.axis_index("kv")
     key_order = shard_index * piece_count + jnp.arange(piece_count, dtype=jnp.int32)
     cache_rows = cache_keys.shape[0]

time: 276 us -> 292 us (1.058); the launches traced: 275 us -> 287 us
  waiting for transfers between devices: 73.9 us -> 95.8 us
  between operations: 17.5 us -> 4.16 us
  starting transfers between devices: 31.2 us -> 38.3 us
  blocking collectives: 53.2 us -> 48.2 us
    all_to_all x0 -> x1, waiting for transfers between devices: none -> 38.9 us  [shards(): shards_2 = lax.all_to_all(shards_2, 'kv', split_axis=0, concat_axis=0)]
    all_gather x1 -> x0, waiting for transfers between devices: 31 us -> none  [shards(): all_queries = lax.all_gather(piece_queries, 'kv', axis=0, tiled=True)]
    all_gather x1, blocking collectives: 31.1 us -> 17.7 us  [sent_together(): lax.all_gather(both, axis, axis=dim, tiled=True)]
    all_to_all x1, waiting for transfers between devices: 28.7 us -> 40.4 us  [sent_and_summed(): lax.all_to_all(cut_along(shard, dim, devices), axis, 0, 0, tiled=True)]
    all_to_all x1, blocking collectives: 22.1 us -> 30.5 us  [from_everyone(): lax.all_to_all(jnp.broadcast_to(shard[None], (devices, *shard.shape)), ax...]
    all_to_all x0 -> x1, starting transfers between devices: none -> 5.23 us  [shards(): shards_2 = lax.all_to_all(shards_2, 'kv', split_axis=0, concat_axis=0)]
  transfers between devices with their start and end apart: 4 -> 4, of which waited for: 4 -> 4; matrix products, arithmetic and copies ran while one was open for 6% -> 5% of each run, Pallas kernels for 0% -> 0%
where the time goes in v1:
time: 292 us; the launch traced here: 287 us
  waiting for transfers between devices  95.8 us (33%)
  matrix products  61.5 us (21%)
  blocking collectives  48.2 us (17%)
  starting transfers between devices  38.3 us (13%)
  other arithmetic  29.4 us (10%)
  local copies, waits for them, and re-layouts  9.48 us (3%)
  between operations  4.16 us (1%)
    all_to_all x1, waiting for transfers between devices, sent_and_summed(): lax.all_to_all(cut_along(shard, dim, devices), axis, 0, 0, tiled=True)  40.4 us
    all_to_all x1, waiting for transfers between devices, shards(): shards_2 = lax.all_to_all(shards_2, 'kv', split_axis=0, concat_axis=0)  38.9 us
    all_to_all x1, blocking collectives, from_everyone(): lax.all_to_all(jnp.broadcast_to(shard[None], (devices, *shard.shape)), ax...  30.5 us
    all_to_all x1, starting transfers between devices, from_everyone(): lax.all_to_all(jnp.broadcast_to(shard[None], (devices, *shard.shape)), ax...  22.4 us
    dot_general x8, matrix products, block_terms(): jnp.einsum('qhd,khd->hqk', query_block, cache_key_heads, preferred_elemen...  18.1 us
    all_gather x1, blocking collectives, sent_together(): lax.all_gather(both, axis, axis=dim, tiled=True)  17.7 us
    reduce_sum x16, other arithmetic, block_terms(): denominator = jnp.sum(cache_exp, axis=-1) + jnp.sum(piece_exp, axis=-1)  17.3 us
    dot_general x8, matrix products, block_terms(): jnp.einsum('hqk,khd->qhd', cache_exp.astype(jnp.bfloat16), cache_value_he...  13.8 us
  transfers between devices with their start and end apart: 4, of which 4 were waited for; matrix products, arithmetic and copies ran while one was open for 5% of the time, Pallas kernels for 0%

profile of v1, /device:TPU:161, one launch (start us, length us, event | category | flops | bytes accessed | tf_op | source)
XLA Modules:
  0.0 287.3 jit_solution(6876971795829406983)
XLA Ops:
  0.7 1.7 fusion.28
  3.0 1.7 fusion.59
  8.6 22.4 %all-to-all-start.1 = ((f32[16,1,1]{2,1,0:T(1,128)}), f32[16,1,1]{2,1,0:T(1,128)S(1)}, u32[]{:S(2)}, u32[]{:S(2)}) async-start(f32[16,1,1]{2,1,0:T(1,128)} %broadcast_in_dim.35), calls=%async_computation.1 | async-start | bytes 16384 | tf_op jit(solution)/shard_map/all_to_all | solution.py:12
  30.9 1.5 convolution_convert_fusion.3
  32.5 8.6 %all-to-all-done.1 = f32[16,1,1]{2,1,0:T(1,128)S(1)} async-done(((f32[16,1,1]{2,1,0:T(1,128)}), f32[16,1,1]{2,1,0:T(1,128)S(1)}, u32[]{:S(2)}, u32[]{:S(2)}) %all-to-all-start.1) | async-done | bytes 96 | tf_op jit(solution)/shard_map/all_to_all | solution.py:12
  41.1 1.2 stack.2
  42.3 5.2 %all-to-all-start = ((bf16[16,256,128]{2,1,0:T(8,128)(2,1)}), bf16[16,256,128]{2,1,0:T(8,128)(2,1)}, u32[]{:S(2)}, u32[]{:S(2)}) async-start(bf16[16,256,128]{2,1,0:T(8,128)(2,1)} %stack.2), calls=%async_computation | async-start | bytes 2097152 | tf_op jit(solution)/shard_map/all_to_all | solution.py:127
  47.6 1.9 convolution_convert_fusion.1
  49.5 1.9 convolution_convert_fusion.2
  54.1 38.9 %all-to-all-done = bf16[16,256,128]{2,1,0:T(8,128)(2,1)} async-done(((bf16[16,256,128]{2,1,0:T(8,128)(2,1)}), bf16[16,256,128]{2,1,0:T(8,128)(2,1)}, u32[]{:S(2)}, u32[]{:S(2)}) %all-to-all-start) | async-done | bytes 1048608 | tf_op jit(solution)/shard_map/all_to_all | solution.py:127
  93.1 76.5 %while.15 = (s32[]{:T(128)}, bf16[8,512,1,128]{3,1,2,0:T(8,128)(2,1)}, f32[8,512,1]{1,2,0:T(1,128)S(1)}, f32[8,512,1]{1,2,0:T(1,128)S(1)}, bf16[8,512,1,128]{3,1...) while((s32[]{:T(128)}, ...), condition=%wide.region_8.9_spmd.clone, body=%wide.region_3.8_spmd.clone.sunk | while | flops 1165229824 | bytes 34173624 | solution.py:179
  95.5 2.3 fusion.96
  97.8 2.1 fusion.100
  100.0 1.7 fusion.98
  105.0 2.3 fusion.96
  107.3 2.1 fusion.100
  109.5 1.7 fusion.98
  113.4 1.2 fusion.97
  114.6 2.3 fusion.96
  116.9 2.1 fusion.100
  119.1 1.7 fusion.98
  123.0 1.2 fusion.97
  124.2 2.3 fusion.96
  126.5 2.1 fusion.100
  128.7 1.7 fusion.98
  132.6 1.2 fusion.97
  133.8 2.3 fusion.96
  136.0 2.1 fusion.100
  138.2 1.7 fusion.98
  142.2 1.2 fusion.97
  143.3 2.3 fusion.96
  145.6 2.1 fusion.100
  147.8 1.7 fusion.98
  152.9 2.3 fusion.96
  155.2 2.1 fusion.100
  157.4 1.7 fusion.98
  162.5 2.3 fusion.96
  164.7 2.1 fusion.100
  166.9 1.7 fusion.98
  169.8 30.5 %all_to_all.29 = f32[16,4096,1]{1,2,0:T(1,128)S(1)} all-to-all(f32[16,4096,1]{1,2,0:T(1,128)S(1)} %broadcast_in_dim.37), channel_id=1, replica_groups=mesh['grp'=2,'kv'=16,'tp'=8] {'kv'}, dimensions={0} | all-to-all | bytes 524288 | tf_op jit(solution)/shard_map/all_to_all | solution.py:12
  201.1 6.2 %all-to-all-start.4 = ((f32[16,256,1]{1,2,0:T(1,128)}), f32[16,256,1]{1,2,0:T(1,128)S(1)}, u32[]{:S(2)}, u32[]{:S(2)}) async-start(f32[16,256,1]{1,2,0:T(1,128)} %bitcast.104), calls=%async_computation.4 | async-start | bytes 32768 | tf_op jit(solution)/shard_map/all_to_all | solution.py:56
  207.3 2.5 fusion.31
  209.9 7.8 %all-to-all-done.4 = f32[16,256,1]{1,2,0:T(1,128)S(1)} async-done(((f32[16,256,1]{1,2,0:T(1,128)}), f32[16,256,1]{1,2,0:T(1,128)S(1)}, u32[]{:S(2)}, u32[]{:S(2)}) %all-to-all-start.4) | async-done | bytes 16416 | tf_op jit(solution)/shard_map/all_to_all | solution.py:56
  217.7 4.5 %all-to-all-start.3 = ((bf16[16,256,128]{2,1,0:T(8,128)(2,1)}), bf16[16,256,128]{2,1,0:T(8,128)(2,1)S(1)}, u32[]{:S(2)}, u32[]{:S(2)}) async-start(bf16[16,256,128]{2,1,0:T(8,128)(2,1)} %bitcast.18), calls=%async_computation.3 | async-start | bytes 2097152 | tf_op jit(solution)/shard_map/all_to_all | solution.py:50
  222.5 1.3 convolution_convert_fusion.7
  223.9 1.3 fusion.38
  227.2 40.4 %all-to-all-done.3 = bf16[16,256,128]{2,1,0:T(8,128)(2,1)S(1)} async-done(((bf16[16,256,128]{2,1,0:T(8,128)(2,1)}), bf16[16,256,128]{2,1,0:T(8,128)(2,1)S(1)}, u32[]{:S(2)}, u32[]{:S(2)}) %all-to-all-start.3) | async-done | bytes 1048608 | tf_op jit(solution)/shard_map/all_to_all | solution.py:50
  267.9 17.7 %all_gather.3 = bf16[260,1024]{1,0:T(8,128)(2,1)S(1)} all-gather(bf16[260,128]{1,0:T(8,128)(2,1)S(1)} %pad_maximum_fusion), channel_id=1, replica_groups=mesh['grp'=2,'kv'=16,'tp'=8] {'tp'}, dimensions={1}, use_global_device_ids=true | all-gather | bytes 599040 | tf_op jit(solution)/shard_map/all_gather | solution.py:62
  (161 shorter events, 32.4 us)
Async XLA Ops:
  0.6 224.7 %copy-start = (bf16[4,2048,128]{2,1,0:T(8,128)(2,1)S(1)}, bf16[4,2048,128]{2,1,0:T(8,128)(2,1)}, u32[]{:S(2)}) copy-start(bf16[4,2048,128]{2,1,0:T(8,128)(2,1)} %param.30) | copy-start | bytes 6291460
  0.6 30.3 %copy-start.5 = (bf16[256,2048]{1,0:T(8,128)(2,1)S(1)}, bf16[256,2048]{1,0:T(8,128)(2,1)}, u32[]{:S(2)}) copy-start(bf16[256,2048]{1,0:T(8,128)(2,1)} %param.18) | copy-start | bytes 3145732
  0.7 30.3 %copy-start.9 = (f32[2048]{0:T(1024)S(1)}, f32[2048]{0:T(1024)}, u32[]{:S(2)}) copy-start(f32[2048]{0:T(1024)} %param.20) | copy-start | bytes 24580
  8.6 32.6 %all-to-all-start.1 = ((f32[16,1,1]{2,1,0:T(1,128)}), f32[16,1,1]{2,1,0:T(1,128)S(1)}, u32[]{:S(2)}, u32[]{:S(2)}) async-start(f32[16,1,1]{2,1,0:T(1,128)} %broadcast_in_dim.35), calls=%async_computation.1 | async-start | bytes 16384 | tf_op jit(solution)/shard_map/all_to_all | solution.py:12
  42.3 50.7 %all-to-all-start = ((bf16[16,256,128]{2,1,0:T(8,128)(2,1)}), bf16[16,256,128]{2,1,0:T(8,128)(2,1)}, u32[]{:S(2)}, u32[]{:S(2)}) async-start(bf16[16,256,128]{2,1,0:T(8,128)(2,1)} %stack.2), calls=%async_computation | async-start | bytes 2097152 | tf_op jit(solution)/shard_map/all_to_all | solution.py:127
  47.6 45.5 %copy-start.1 = (bf16[4096,128]{1,0:T(8,128)(2,1)S(1)}, bf16[4096,128]{1,0:T(8,128)(2,1)}, u32[]{:S(2)}) copy-start(bf16[4096,128]{1,0:T(8,128)(2,1)} %param.27) | copy-start | bytes 3145732
  47.6 45.5 %copy-start.2 = (f32[1,4096]{1,0:T(1,128)S(1)}, f32[1,4096]{1,0:T(1,128)}, u32[]{:S(2)}) copy-start(f32[1,4096]{1,0:T(1,128)} %param.29) | copy-start | bytes 49156
  97.7 2.2 copy-start.11
  107.3 2.2 copy-start.11
  116.9 2.2 copy-start.11
  126.5 2.2 copy-start.11
  136.0 2.2 copy-start.11
  145.6 2.2 copy-start.11
  155.2 2.2 copy-start.11
  164.7 2.2 copy-start.11
  169.6 48.1 %copy-start.4 = (bf16[256,1,128]{2,0,1:T(8,128)(2,1)}, bf16[256,1,128]{2,0,1:T(8,128)(2,1)S(1)}, u32[]{:S(2)}) copy-start(bf16[256,1,128]{2,0,1:T(8,128)(2,1)S(1)} %get-tuple-element.329) | copy-start | bytes 196612
  169.6 48.1 %copy-start.14 = (bf16[256,1,128]{2,0,1:T(8,128)(2,1)}, bf16[256,1,128]{2,0,1:T(8,128)(2,1)S(1)}, u32[]{:S(2)}) copy-start(bf16[256,1,128]{2,0,1:T(8,128)(2,1)S(1)} %get-tuple-element.332) | copy-start | bytes 196612
  201.1 16.6 %all-to-all-start.4 = ((f32[16,256,1]{1,2,0:T(1,128)}), f32[16,256,1]{1,2,0:T(1,128)S(1)}, u32[]{:S(2)}, u32[]{:S(2)}) async-start(f32[16,256,1]{1,2,0:T(1,128)} %bitcast.104), calls=%async_computation.4 | async-start | bytes 32768 | tf_op jit(solution)/shard_map/all_to_all | solution.py:56
  207.3 15.0 %copy-start.7 = (bf16[4,2048]{1,0:T(4,128)(2,1)S(1)}, bf16[4,2048]{1,0:T(4,128)(2,1)}, u32[]{:S(2)}) copy-start(bf16[4,2048]{1,0:T(4,128)(2,1)} %param.19) | copy-start | bytes 49156
  209.9 15.4 %copy-start.13 = (bf16[2048,1]{0,1:T(2,128)(2,1)S(1)}, bf16[2048,1]{0,1:T(2,128)(2,1)}, u32[]{:S(2)}) copy-start(bf16[2048,1]{0,1:T(2,128)(2,1)} %param.24) | copy-start | bytes 12292
  217.7 49.9 %all-to-all-start.3 = ((bf16[16,256,128]{2,1,0:T(8,128)(2,1)}), bf16[16,256,128]{2,1,0:T(8,128)(2,1)S(1)}, u32[]{:S(2)}, u32[]{:S(2)}) async-start(bf16[16,256,128]{2,1,0:T(8,128)(2,1)} %bitcast.18), calls=%async_computation.3 | async-start | bytes 2097152 | tf_op jit(solution)/shard_map/all_to_all | solution.py:50
  222.3 3.8 %copy-start.8 = (f32[4,1,2048]{2,1,0:T(1,128)S(1)}, f32[4,1,2048]{2,1,0:T(1,128)}, u32[]{:S(2)}) copy-start(f32[4,1,2048]{2,1,0:T(1,128)} %param.32) | copy-start | bytes 98308
  222.3 3.8 %copy-start.10 = (s32[4]{0:T(128)S(1)}, s32[4]{0:T(128)}, u32[]{:S(2)}) copy-start(s32[4]{0:T(128)} %param.33) | copy-start | bytes 52
  222.3 4.2 %copy-start.3 = (bf16[4,2048,128]{2,1,0:T(8,128)(2,1)S(1)}, bf16[4,2048,128]{2,1,0:T(8,128)(2,1)}, u32[]{:S(2)}) copy-start(bf16[4,2048,128]{2,1,0:T(8,128)(2,1)} %param.31) | copy-start | bytes 6291460
  225.4 1.6 copy-start.12
  267.6 18.0 %copy-start.6 = (bf16[1024,256]{1,0:T(8,128)(2,1)S(1)}, bf16[1024,256]{1,0:T(8,128)(2,1)}, u32[]{:S(2)}) copy-start(bf16[1024,256]{1,0:T(8,128)(2,1)} %param.26) | copy-start | bytes 1572868
